TPU v7x, 512 devices: a 4x2x32 block of a 4x8x32 slice. The times are simulated.
512 devices in a mesh: grp: 2 (over y), fs: 32 (over z), tp: 8 (over x, core).
Axes of the slice: x: 4, y: 2, z: 32, core: 2. Of those that a mesh axis runs over, the one named last changes fastest.
The devices are a block of a 4x8x32 slice.
Arguments:
- tokens: bfloat16 [24576, 2048], P(('grp', 'fs'), 'tp'), parts along dimension 0, may hold values from -6 to 6
- mix_gain: float32 [2048], replicated, may hold values from 0.1 to 1.9
- w_signal: bfloat16 [2048, 1024], P('fs', 'tp'), may hold values from -0.125 to 0.125
- w_outer_gate: bfloat16 [2048, 1024], P('fs', 'tp'), may hold values from -0.125 to 0.125
- w_inner_gate: bfloat16 [2048, 1024], P('fs', 'tp'), may hold values from -0.125 to 0.125
- mix_taps: float32 [3, 1024], P(None, 'tp'), may hold values from -3 to 3
- w_mix_out: bfloat16 [1024, 2048], P('tp', 'fs'), may hold values from -0.1875 to 0.1875
- ffn_gain: float32 [2048], replicated, may hold values from 0.1 to 1.9
- w_gate: bfloat16 [2048, 5120], P('fs', 'tp'), may hold values from -0.125 to 0.125
- w_value: bfloat16 [2048, 5120], P('fs', 'tp'), may hold values from -0.125 to 0.125
- up_taps: float32 [2, 3, 5120], P(None, None, 'tp'), may hold values from -3 to 3
- up_bias: float32 [2, 5120], P(None, 'tp'), may hold values from -3 to 3
- w_down: bfloat16 [5120, 2048], P('tp', 'fs'), may hold values from -0.078125 to 0.078125
Outputs:
- layer_out: bfloat16 [24576, 2048], P(('grp', 'fs'), 'tp'), parts along dimension 0
There are 2 independent parts, one for each index of `grp`. A program takes and returns all parts, laid end to end along the dimension named above; an argument that names none is the same for every part. Nothing has to cross between parts.
All inputs are finite; a program needn't handle non-finite values.
Results may differ from a plain program's by a relative error of at most 0.022.
Values may be sent and summed in bfloat16 or wider, within the bound.
A program may use at most 64 MiB of HBM per device.

v0:
```python
import jax
import jax.numpy as jnp
from jax import lax
from jax.sharding import PartitionSpec as P

SEQS_DEV = 2


def in_one_piece(arrays, axis, dim, along):
    widths = [a.shape[along] for a in arrays]
    both = jnp.concatenate(arrays, axis=along)
    filled = lax.all_gather(both, axis, axis=dim, tiled=True)
    return tuple(jnp.split(filled, [sum(widths[:k]) for k in range(1, len(widths))], axis=along))


def copy_for_each(value, axis):
    copies = jnp.broadcast_to(value, (lax.axis_size(axis), *value.shape))
    return lax.all_to_all(copies, axis, split_axis=0, concat_axis=0, tiled=True)


def in_order(pieces, dim):
    shape = list(pieces.shape[1:])
    shape[dim] *= pieces.shape[0]
    return jnp.moveaxis(pieces, 0, dim).reshape(shape)


def gathered_copies(value, axis, dim):
    pieces = copy_for_each(value, axis)
    return in_order(pieces, dim)


def split_up(value, dim, devices):
    shape = value.shape
    pieces = value.reshape(*shape[:dim], devices, shape[dim] // devices, *shape[dim + 1 :])
    return jnp.moveaxis(pieces, dim, 0)


def sent_and_summed(value, axis, dim):
    devices = lax.axis_size(axis)
    pieces = lax.all_to_all(split_up(value, dim, devices), axis, 0, 0, tiled=True)
    return jnp.sum(pieces.astype(jnp.float32), axis=0)


def conv_positions(values, taps):
    width = values.shape[1]
    blocks = values.reshape(SEQS_DEV, -1, width)
    length = blocks.shape[1]
    padded = jnp.pad(blocks, ((0, 0), (2, 0), (0, 0)))
    result = (
        padded[:, 0:length] * taps[0]
        + padded[:, 1 : length + 1] * taps[1]
        + padded[:, 2 : length + 2] * taps[2]
    )
    return result.reshape(-1, width)


def rms_norm(stream, gain):
    values = stream.astype(jnp.float32)
    scale = lax.rsqrt(jnp.mean(values * values, axis=-1, keepdims=True) + 1e-06)
    return (values * scale * gain).astype(jnp.bfloat16)


def on_device(
    tokens,
    mix_gain,
    w_signal,
    w_outer_gate,
    w_inner_gate,
    mix_taps,
    w_mix_out,
    ffn_gain,
    w_gate,
    w_value,
    up_taps,
    up_bias,
    w_down,
):
    gate_full, value_full = in_one_piece((w_gate, w_value), "fs", 0, 1)
    whole = gathered_copies(tokens, "tp", 1)
    normed = rms_norm(whole, mix_gain)
    signal_full, outer_full, inner_full = in_one_piece(
        (w_signal, w_outer_gate, w_inner_gate), "fs", 0, 1
    )
    signal = jnp.dot(normed, signal_full, preferred_element_type=jnp.float32)
    outer = jnp.dot(normed, outer_full, preferred_element_type=jnp.float32)
    inner = jnp.dot(normed, inner_full, preferred_element_type=jnp.float32)
    signal = signal.astype(jnp.bfloat16).astype(jnp.float32)
    outer = outer.astype(jnp.bfloat16).astype(jnp.float32)
    inner = inner.astype(jnp.bfloat16).astype(jnp.float32)
    mixed = (outer * conv_positions(inner * signal, mix_taps)).astype(jnp.bfloat16)
    mix_terms = jnp.dot(
        mixed,
        lax.all_gather(w_mix_out, "fs", axis=1, tiled=True),
        preferred_element_type=jnp.float32,
    )
    mix_sum = sent_and_summed(mix_terms.astype(jnp.bfloat16), "tp", 1)
    resid = (tokens.astype(jnp.float32) + mix_sum).astype(jnp.bfloat16)
    whole_ffn = gathered_copies(resid, "tp", 1)
    normed_ffn = rms_norm(whole_ffn, ffn_gain)
    gate = jnp.dot(normed_ffn, gate_full, preferred_element_type=jnp.float32)
    value = jnp.dot(normed_ffn, value_full, preferred_element_type=jnp.float32)
    gate = gate.astype(jnp.bfloat16).astype(jnp.float32)
    value = value.astype(jnp.bfloat16).astype(jnp.float32)
    gate_conv = conv_positions(gate, up_taps[0]) + up_bias[0]
    value_conv = conv_positions(value, up_taps[1]) + up_bias[1]
    hidden = (jax.nn.silu(gate_conv) * value_conv).astype(jnp.bfloat16)
    ffn_terms = jnp.dot(
        hidden, lax.all_gather(w_down, "fs", axis=1, tiled=True), preferred_element_type=jnp.float32
    )
    ffn_sum = sent_and_summed(ffn_terms.astype(jnp.bfloat16), "tp", 1)
    return (resid.astype(jnp.float32) + ffn_sum).astype(jnp.bfloat16)


def solution(mesh):
    placed = (
        P(("grp", "fs"), "tp"),
        P(),
        P("fs", "tp"),
        P("fs", "tp"),
        P("fs", "tp"),
        P(None, "tp"),
        P("tp", "fs"),
        P(),
        P("fs", "tp"),
        P("fs", "tp"),
        P(None, None, "tp"),
        P(None, "tp"),
        P("tp", "fs"),
    )
    return jax.shard_map(
        on_device, mesh=mesh, in_specs=placed, out_specs=P(("grp", "fs"), "tp"), check_vma=False
    )
```

profile of v0, /device:TPU:33, one launch (start us, length us, event | category | flops | bytes accessed | tf_op | source)
XLA Modules:
  0.0 474.6 jit_solution(4301556435789790506)
XLA Ops:
  6.5 0.0 all-gather.4.cloned.1.call-start
  6.6 1.4 pad_maximum_fusion.1
  7.9 0.1 all-gather.4.cloned.1.call-update
  8.0 0.1 all-gather.6.cloned.1.call-start
  8.1 1.6 pad_maximum_fusion
  9.7 0.1 all-gather.6.cloned.1.call-update
  9.7 1.1 copy.16
  10.8 1.3 broadcast_in_dim.4
  12.1 0.0 copy-start.6
  12.1 0.0 copy-start.1
  12.1 45.1 %all-to-all-start = ((bf16[8,384,256]{1,2,0:T(8,128)(2,1)}), bf16[8,384,256]{1,2,0:T(8,128)(2,1)S(1)}, u32[]{:S(2)}, u32[]{:S(2)}) async-start(bf16[8,384,256]{1,2,0:T(8,128)(2,1)} %broadcast_in_dim.4), calls=%async_computation | async-start | bytes 3145728 | tf_op jit(solution)/shard_map/all_to_all | solution.py:18
  57.2 0.0 copy-done.6
  57.2 0.0 copy-start.3
  57.2 0.0 copy-done.1
  57.2 52.2 %all_gather.13 = bf16[128,2048]{0,1:T(8,128)(2,1)} all-gather(bf16[128,64]{0,1:T(8,128)(2,1)S(1)} %copy-done.1), channel_id=1, replica_groups=mesh['grp'=2,'fs'=32,'tp'=8] {'fs'}, dimensions={1}, use_global_device_ids=true | all-gather | bytes 540672 | tf_op jit(solution)/shard_map/all_gather | solution.py:93
  109.4 0.0 all-to-all-done
  109.4 0.4 multiply_reduce_fusion.1
  109.9 0.0 copy-done.3
  109.9 0.4 fusion.3
  110.3 39.8 %all-gather.4.cloned.1.call-done = bf16[2048,384]{1,0:T(8,128)(2,1)} async-done(((bf16[64,384]{1,0:T(8,128)(2,1)}), bf16[2048,384]{1,0:T(8,128)(2,1)}) %all-gather.4.cloned.1.call-update) | async-done | bytes 1572880 | tf_op jit(solution)/shard_map/all_gather | solution.py:12
  150.0 1.7 fusion.16
  151.7 1.7 fusion.15
  153.4 0.1 fusion.36
  153.5 3.0 convolution_convert_fusion.1
  156.5 1.3 copy.25
  157.8 25.3 %all-to-all-start.1 = ((bf16[8,384,256]{2,1,0:T(8,128)(2,1)}), bf16[8,384,256]{2,1,0:T(8,128)(2,1)S(1)}, u32[]{:S(2)}, u32[]{:S(2)}) async-start(bf16[8,384,256]{2,1,0:T(8,128)(2,1)} %bitcast.59), calls=%async_computation.1 | async-start | bytes 3145728 | tf_op jit(solution)/shard_map/all_to_all | solution.py:40
  183.1 0.0 copy-start
  183.1 0.0 all-gather.8.cloned.1.call-start
  183.1 0.7 all-gather.8.cloned.1.call-update
  183.9 19.8 %all-to-all-done.1 = bf16[8,384,256]{2,1,0:T(8,128)(2,1)S(1)} async-done(((bf16[8,384,256]{2,1,0:T(8,128)(2,1)}), bf16[8,384,256]{2,1,0:T(8,128)(2,1)S(1)}, u32[]{:S(2)}, u32[]{:S(2)}) %all-to-all-start.1) | async-done | bytes 1572896 | tf_op jit(solution)/shard_map/all_to_all | solution.py:40
  203.7 0.2 convert_reduce_fusion.1
  203.9 0.0 copy-done
  203.9 0.1 add_convert_fusion.1
  204.0 0.2 copy.18
  204.2 1.4 broadcast_in_dim.5
  205.5 0.0 copy-start.5
  205.5 0.0 copy-start.2
  205.5 4.6 all-to-all-start.2
  210.1 0.0 copy-done.5
  210.1 0.0 copy-start.4
  210.2 0.0 copy-done.2
  210.2 20.6 %all-to-all-done.2 = bf16[8,384,256]{1,2,0:T(8,128)(2,1)S(1)} async-done(((bf16[8,384,256]{1,2,0:T(8,128)(2,1)}), bf16[8,384,256]{1,2,0:T(8,128)(2,1)S(1)}, u32[]{:S(2)}, u32[]{:S(2)}) %all-to-all-start.2) | async-done | bytes 1572896 | tf_op jit(solution)/shard_map/all_to_all | solution.py:18
  230.8 0.4 multiply_reduce_fusion
  231.2 0.0 copy-done.4
  231.3 0.4 fusion.1
  231.7 56.5 %all-gather.6.cloned.1.call-done = bf16[2048,1280]{1,0:T(8,128)(2,1)} async-done(((bf16[64,1280]{1,0:T(8,128)(2,1)}), bf16[2048,1280]{1,0:T(8,128)(2,1)}) %all-gather.6.cloned.1.call-update) | async-done | bytes 5242896 | tf_op jit(solution)/shard_map/all_gather | solution.py:12
  288.2 0.0 copy-start.7
  288.2 3.3 fusion.8
  291.5 0.1 convert.6
  291.6 0.0 copy-done.7
  291.6 1.4 fusion.11
  293.0 0.1 convert.7
  293.1 0.6 fusion.22
  293.7 0.3 fusion.29
  294.0 124.1 %all-gather.8.cloned.1.call-done = bf16[640,2048]{0,1:T(8,128)(2,1)} async-done(((bf16[640,64]{0,1:T(8,128)(2,1)}), bf16[640,2048]{0,1:T(8,128)(2,1)}) %all-gather.8.cloned.1.call-update) | async-done | bytes 2621456 | tf_op jit(solution)/shard_map/all_gather | solution.py:108
  418.1 3.2 convolution_convert_fusion
  421.3 0.1 copy.24
  421.4 45.7 %all_to_all.20 = bf16[8,384,256]{2,1,0:T(8,128)(2,1)S(1)} all-to-all(bf16[8,384,256]{2,1,0:T(8,128)(2,1)S(1)} %bitcast.61), channel_id=1, replica_groups=mesh['grp'=2,'fs'=32,'tp'=8] {'tp'}, dimensions={0} | all-to-all | bytes 3145728 | tf_op jit(solution)/shard_map/all_to_all | solution.py:40
  467.1 0.2 convert_reduce_fusion
  467.3 0.7 add_convert_fusion
  (5 shorter events, 0.1 us)
Async XLA Ops:
  6.5 143.5 %all-gather.4.cloned.1.call-start = ((), (), s32[]{:S(2)}) async-start(), calls=%async_computation.4 | async-start | bytes 1622016 | tf_op jit(solution)/shard_map/all_gather | solution.py:12
  8.0 280.2 %all-gather.6.cloned.1.call-start = ((), (), s32[]{:S(2)}) async-start(), calls=%async_computation.5 | async-start | bytes 5406720 | tf_op jit(solution)/shard_map/all_gather | solution.py:12
  12.1 45.1 %copy-start.6 = (f32[3,128]{1,0:T(4,128)S(1)}, f32[3,128]{1,0:T(4,128)}, u32[]{:S(2)}) copy-start(f32[3,128]{1,0:T(4,128)} %param.18) | copy-start | bytes 4612
  12.1 45.1 %copy-start.1 = (bf16[128,64]{0,1:T(8,128)(2,1)S(1)}, bf16[128,64]{0,1:T(8,128)(2,1)}, u32[]{:S(2)}) copy-start(bf16[128,64]{0,1:T(8,128)(2,1)} %param.19) | copy-start | bytes 49156
  12.1 97.3 %all-to-all-start = ((bf16[8,384,256]{1,2,0:T(8,128)(2,1)}), bf16[8,384,256]{1,2,0:T(8,128)(2,1)S(1)}, u32[]{:S(2)}, u32[]{:S(2)}) async-start(bf16[8,384,256]{1,2,0:T(8,128)(2,1)} %broadcast_in_dim.4), calls=%async_computation | async-start | bytes 3145728 | tf_op jit(solution)/shard_map/all_to_all | solution.py:18
  57.2 52.7 %copy-start.3 = (f32[2048]{0:T(1024)S(1)}, f32[2048]{0:T(1024)}, u32[]{:S(2)}) copy-start(f32[2048]{0:T(1024)} %param.14) | copy-start | bytes 24580
  157.8 45.9 %all-to-all-start.1 = ((bf16[8,384,256]{2,1,0:T(8,128)(2,1)}), bf16[8,384,256]{2,1,0:T(8,128)(2,1)S(1)}, u32[]{:S(2)}, u32[]{:S(2)}) async-start(bf16[8,384,256]{2,1,0:T(8,128)(2,1)} %bitcast.59), calls=%async_computation.1 | async-start | bytes 3145728 | tf_op jit(solution)/shard_map/all_to_all | solution.py:40
  183.1 20.8 %copy-start = (bf16[384,256]{1,0:T(8,128)(2,1)S(1)}, bf16[384,256]{1,0:T(8,128)(2,1)}, u32[]{:S(2)}) copy-start(bf16[384,256]{1,0:T(8,128)(2,1)} %param.13) | copy-start | bytes 589828
  183.1 235.0 %all-gather.8.cloned.1.call-start = ((), (), s32[]{:S(2)}) async-start(), calls=%async_computation.6 | async-start | bytes 2703360 | tf_op jit(solution)/shard_map/all_gather | solution.py:108
  205.5 4.6 copy-start.5
  205.5 4.6 copy-start.2
  205.5 25.3 %all-to-all-start.2 = ((bf16[8,384,256]{1,2,0:T(8,128)(2,1)}), bf16[8,384,256]{1,2,0:T(8,128)(2,1)S(1)}, u32[]{:S(2)}, u32[]{:S(2)}) async-start(bf16[8,384,256]{1,2,0:T(8,128)(2,1)} %broadcast_in_dim.5), calls=%async_computation.2 | async-start | bytes 3145728 | tf_op jit(solution)/shard_map/all_to_all | solution.py:18
  210.1 21.1 %copy-start.4 = (f32[2048]{0:T(1024)S(1)}, f32[2048]{0:T(1024)}, u32[]{:S(2)}) copy-start(f32[2048]{0:T(1024)} %param.20) | copy-start | bytes 24580
  288.2 3.4 copy-start.7
Sparse Core Ops, SparseCore 0:
  9.4 140.5 all-gather.3
  152.1 135.9 all-gather.5
  290.3 127.7 all-gather.7
where the time goes:
time: 475 us
  waiting for transfers between devices  262 us (55%)
  blocking collectives  98 us (21%)
  starting transfers between devices  75.1 us (16%)
  matrix products  14.3 us (3%)
  between operations  13.3 us (3%)
  other arithmetic  6.94 us (1%)
  local copies, waits for them, and re-layouts  5.44 us (1%)
    all_gather x1, waiting for transfers between devices, on_device(): lax.all_gather(w_down, 'fs', axis=1, tiled=True)  124 us
    all_gather x2, waiting for transfers between devices, in_one_piece(): filled = lax.all_gather(both, axis, axis=dim, tiled=True)  96.2 us
    all_gather x1, blocking collectives, on_device(): lax.all_gather(w_mix_out, 'fs', axis=1, tiled=True)  52.2 us
    all_to_all x2, starting transfers between devices, copy_for_each(): return lax.all_to_all(copies, axis, split_axis=0, concat_axis=0, tiled=True)  49.7 us
    all_to_all x1, blocking collectives, sent_and_summed(): lax.all_to_all(split_up(value, dim, devices), axis, 0, 0, tiled=True)  45.7 us
    all_to_all x1, starting transfers between devices, sent_and_summed(): lax.all_to_all(split_up(value, dim, devices), axis, 0, 0, tiled=True)  25.3 us
    all_to_all x2, waiting for transfers between devices, copy_for_each(): return lax.all_to_all(copies, axis, split_axis=0, concat_axis=0, tiled=True)  20.6 us
    all_to_all x1, waiting for transfers between devices, sent_and_summed(): lax.all_to_all(split_up(value, dim, devices), axis, 0, 0, tiled=True)  19.8 us
  transfers between devices with their start and end apart: 6, of which 5 were waited for; matrix products, arithmetic and copies ran while one was open for 4% of the time, Pallas kernels for 0%

commit v1 on v0

--- a/solution.py
+++ b/solution.py
@@ -104,9 +104,16 @@
     gate_conv = conv_positions(gate, up_taps[0]) + up_bias[0]
     value_conv = conv_positions(value, up_taps[1]) + up_bias[1]
     hidden = (jax.nn.silu(gate_conv) * value_conv).astype(jnp.bfloat16)
-    ffn_terms = jnp.dot(
-        hidden, lax.all_gather(w_down, "fs", axis=1, tiled=True), preferred_element_type=jnp.float32
+    begin_desk = lambda mine_x, out_dim: jnp.concatenate(
+        lax.all_to_all(
+            jnp.stack([mine_x for _ in range(lax.axis_size("fs"))]),
+            concat_axis=0,
+            split_axis=0,
+            axis_name="fs",
+        ),
+        out_dim,
     )
+    ffn_terms = jnp.dot(hidden, begin_desk(w_down, 1), preferred_element_type=jnp.float32)
     ffn_sum = sent_and_summed(ffn_terms.astype(jnp.bfloat16), "tp", 1)
     return (resid.astype(jnp.float32) + ffn_sum).astype(jnp.bfloat16)
 

time: 475 us -> 603 us (1.27)
  waiting for transfers between devices: 262 us -> 347 us
  blocking collectives: 98 us -> 158 us
  starting transfers between devices: 75.1 us -> 58.3 us
    all_gather x2, waiting for transfers between devices: 96.2 us -> 347 us  [in_one_piece(): filled = lax.all_gather(both, axis, axis=dim, tiled=True)]
    all_gather x1 -> x0, waiting for transfers between devices: 124 us -> none  [on_device(): lax.all_gather(w_down, 'fs', axis=1, tiled=True)]
    all_to_all x1 -> x2, blocking collectives: 45.7 us -> 81.6 us  [sent_and_summed(): lax.all_to_all(split_up(value, dim, devices), axis, 0, 0, tiled=True)]
    all_to_all x0 -> x1, blocking collectives: none -> 24.2 us  [copy_for_each(): return lax.all_to_all(copies, axis, split_axis=0, concat_axis=0, tiled=True)]
    all_to_all x2 -> x1, waiting for transfers between devices: 20.6 us -> 0.01 us  [copy_for_each(): return lax.all_to_all(copies, axis, split_axis=0, concat_axis=0, tiled=True)]
    all_to_all x1, waiting for transfers between devices: 19.8 us -> 0.01 us  [on_device(): lax.all_to_all(jnp.stack([mine_x for _ in range(lax.axis_size('fs'))]), c...]
    all_to_all x1, starting transfers between devices: 25.3 us -> 13 us  [on_device(): lax.all_to_all(jnp.stack([mine_x for _ in range(lax.axis_size('fs'))]), c...]
    all_to_all x2 -> x1, starting transfers between devices: 49.7 us -> 45.1 us  [copy_for_each(): return lax.all_to_all(copies, axis, split_axis=0, concat_axis=0, tiled=True)]
  transfers between devices with their start and end apart: 6 -> 4, of which waited for: 5 -> 2; matrix products, arithmetic and copies ran while one was open for 4% -> 2% of each run, Pallas kernels for 0% -> 0%
where the time goes in v1:
time: 603 us; the launch traced here: 602 us
  waiting for transfers between devices  347 us (58%)
  blocking collectives  158 us (26%)
  starting transfers between devices  58.3 us (10%)
  matrix products  14.3 us (2%)
  between operations  13.7 us (2%)
    all_gather x2, waiting for transfers between devices, in_one_piece(): filled = lax.all_gather(both, axis, axis=dim, tiled=True)  347 us
    all_to_all x2, blocking collectives, sent_and_summed(): lax.all_to_all(split_up(value, dim, devices), axis, 0, 0, tiled=True)  81.6 us
    all_gather x1, blocking collectives, on_device(): lax.all_gather(w_mix_out, 'fs', axis=1, tiled=True)  51.7 us
    all_to_all x1, starting transfers between devices, copy_for_each(): return lax.all_to_all(copies, axis, split_axis=0, concat_axis=0, tiled=True)  45.1 us
    all_to_all x1, blocking collectives, copy_for_each(): return lax.all_to_all(copies, axis, split_axis=0, concat_axis=0, tiled=True)  24.2 us
    all_to_all x1, starting transfers between devices, on_device(): lax.all_to_all(jnp.stack([mine_x for _ in range(lax.axis_size('fs'))]), c...  13 us
  transfers between devices with their start and end apart: 4, of which 2 were waited for; matrix products, arithmetic and copies ran while one was open for 2% of the time, Pallas kernels for 0%

profile of v1, /device:TPU:33, one launch (start us, length us, event | category | flops | bytes accessed | tf_op | source)
XLA Modules:
  0.0 602.4 jit_solution(1533080965248781350)
XLA Ops:
  6.5 0.0 all-gather.3.cloned.1.call-start
  6.6 1.4 pad_maximum_fusion.1
  7.9 0.1 all-gather.3.cloned.1.call-update
  8.0 1.1 copy.17
  9.1 1.3 broadcast_in_dim.4
  10.4 0.0 copy-start.9
  10.4 0.0 copy-start.4
  10.4 45.1 %all-to-all-start = ((bf16[8,384,256]{1,2,0:T(8,128)(2,1)}), bf16[8,384,256]{1,2,0:T(8,128)(2,1)S(1)}, u32[]{:S(2)}, u32[]{:S(2)}) async-start(bf16[8,384,256]{1,2,0:T(8,128)(2,1)} %broadcast_in_dim.4), calls=%async_computation | async-start | bytes 3145728 | tf_op jit(solution)/shard_map/all_to_all | solution.py:18
  55.4 0.0 copy-done.9
  55.4 0.0 copy-start.6
  55.5 0.0 copy-done.4
  55.5 51.7 %all_gather.10 = bf16[128,2048]{0,1:T(8,128)(2,1)} all-gather(bf16[128,64]{0,1:T(8,128)(2,1)S(1)} %copy-done.4), channel_id=1, replica_groups=mesh['grp'=2,'fs'=32,'tp'=8] {'fs'}, dimensions={1}, use_global_device_ids=true | all-gather | bytes 540672 | tf_op jit(solution)/shard_map/all_gather | solution.py:93
  107.2 0.0 all-to-all-done
  107.2 0.4 multiply_reduce_fusion.1
  107.6 0.0 copy-done.6
  107.6 0.4 fusion.3
  108.0 41.5 %all-gather.3.cloned.1.call-done = bf16[2048,384]{1,0:T(8,128)(2,1)} async-done(((bf16[64,384]{1,0:T(8,128)(2,1)}), bf16[2048,384]{1,0:T(8,128)(2,1)}) %all-gather.3.cloned.1.call-update) | async-done | bytes 1572880 | tf_op jit(solution)/shard_map/all_gather | solution.py:12
  149.5 1.7 fusion.16
  151.2 1.7 fusion.15
  152.9 0.1 fusion.38
  152.9 3.0 convolution_convert_fusion.1
  155.9 0.1 copy.26
  156.1 46.7 %all_to_all.25 = bf16[8,384,256]{2,1,0:T(8,128)(2,1)S(1)} all-to-all(bf16[8,384,256]{2,1,0:T(8,128)(2,1)S(1)} %bitcast.55), channel_id=1, replica_groups=mesh['grp'=2,'fs'=32,'tp'=8] {'tp'}, dimensions={0} | all-to-all | bytes 3145728 | tf_op jit(solution)/shard_map/all_to_all | solution.py:40
  202.7 0.0 copy-start
  202.7 0.2 convert_reduce_fusion.1
  202.9 0.7 copy-done
  203.7 0.2 copy.19
  203.9 0.1 broadcast_in_dim.5
  204.0 0.0 copy-start.3
  204.0 24.2 %all_to_all.26 = bf16[8,384,256]{1,2,0:T(8,128)(2,1)S(1)} all-to-all(bf16[8,384,256]{1,2,0:T(8,128)(2,1)S(1)} %broadcast_in_dim.5), channel_id=1, replica_groups=mesh['grp'=2,'fs'=32,'tp'=8] {'tp'}, dimensions={0} | all-to-all | bytes 3145728 | tf_op jit(solution)/shard_map/all_to_all | solution.py:18
  228.3 0.0 copy-done.3
  228.3 1.9 stack.2
  230.2 0.0 copy-start.1
  230.2 0.0 copy-start.2
  230.2 0.0 copy-start.8
  230.2 0.0 copy-start.5
  230.2 13.0 %all-to-all-start.3 = ((bf16[32,640,64]{1,2,0:T(8,128)(2,1)}), bf16[32,640,64]{1,2,0:T(8,128)(2,1)}, u32[]{:S(2)}, u32[]{:S(2)}) async-start(bf16[32,640,64]{1,2,0:T(8,128)(2,1)} %stack.2), calls=%async_computation.3 | async-start | bytes 5242880 | tf_op jit(solution)/shard_map/all_to_all | solution.py:108
  243.2 0.0 copy-start.7
  243.2 0.2 all-gather.5.cloned.1.call-start
  243.4 0.0 copy-done.1
  243.5 0.0 copy-done.2
  243.5 0.7 pad_maximum_fusion
  244.2 0.1 all-gather.5.cloned.1.call-update
  244.2 0.0 copy-done.8
  244.2 0.0 copy-done.5
  244.3 0.4 multiply_reduce_fusion
  244.7 0.0 copy-done.7
  244.7 0.4 fusion.1
  245.2 305.4 %all-gather.5.cloned.1.call-done = bf16[2048,1280]{1,0:T(8,128)(2,1)} async-done(((bf16[64,1280]{1,0:T(8,128)(2,1)}), bf16[2048,1280]{1,0:T(8,128)(2,1)}) %all-gather.5.cloned.1.call-update) | async-done | bytes 5242896 | tf_op jit(solution)/shard_map/all_gather | solution.py:12
  550.6 0.0 copy-start.10
  550.6 3.3 fusion.8
  554.0 0.1 convert.6
  554.0 0.0 copy-done.10
  554.0 1.4 fusion.11
  555.5 0.1 convert.7
  555.6 0.9 fusion.30
  556.4 0.0 all-to-all-done.3
  556.4 3.2 convolution_convert_fusion
  559.6 0.1 copy.25
  559.7 34.9 %all_to_all.27 = bf16[8,384,256]{2,1,0:T(8,128)(2,1)S(1)} all-to-all(bf16[8,384,256]{2,1,0:T(8,128)(2,1)S(1)} %bitcast.56), channel_id=1, replica_groups=mesh['grp'=2,'fs'=32,'tp'=8] {'tp'}, dimensions={0} | all-to-all | bytes 3145728 | tf_op jit(solution)/shard_map/all_to_all | solution.py:40
  594.6 0.2 convert_reduce_fusion
  594.9 0.7 add_convert_fusion
  (6 shorter events, 0.1 us)
Async XLA Ops:
  6.5 143.0 %all-gather.3.cloned.1.call-start = ((), (), s32[]{:S(2)}) async-start(), calls=%async_computation.5 | async-start | bytes 1622016 | tf_op jit(solution)/shard_map/all_gather | solution.py:12
  10.4 45.1 %copy-start.9 = (f32[3,128]{1,0:T(4,128)S(1)}, f32[3,128]{1,0:T(4,128)}, u32[]{:S(2)}) copy-start(f32[3,128]{1,0:T(4,128)} %param.18) | copy-start | bytes 4612
  10.4 45.1 %copy-start.4 = (bf16[128,64]{0,1:T(8,128)(2,1)S(1)}, bf16[128,64]{0,1:T(8,128)(2,1)}, u32[]{:S(2)}) copy-start(bf16[128,64]{0,1:T(8,128)(2,1)} %param.19) | copy-start | bytes 49156
  10.4 96.8 %all-to-all-start = ((bf16[8,384,256]{1,2,0:T(8,128)(2,1)}), bf16[8,384,256]{1,2,0:T(8,128)(2,1)S(1)}, u32[]{:S(2)}, u32[]{:S(2)}) async-start(bf16[8,384,256]{1,2,0:T(8,128)(2,1)} %broadcast_in_dim.4), calls=%async_computation | async-start | bytes 3145728 | tf_op jit(solution)/shard_map/all_to_all | solution.py:18
  55.4 52.2 %copy-start.6 = (f32[2048]{0:T(1024)S(1)}, f32[2048]{0:T(1024)}, u32[]{:S(2)}) copy-start(f32[2048]{0:T(1024)} %param.14) | copy-start | bytes 24580
  202.7 0.9 copy-start
  204.0 24.3 %copy-start.3 = (bf16[640,64]{0,1:T(8,128)(2,1)S(1)}, bf16[640,64]{0,1:T(8,128)(2,1)}, u32[]{:S(2)}) copy-start(bf16[640,64]{0,1:T(8,128)(2,1)} %param.25) | copy-start | bytes 245764
  230.2 13.3 %copy-start.1 = (bf16[64,640]{1,0:T(8,128)(2,1)S(1)}, bf16[64,640]{1,0:T(8,128)(2,1)}, u32[]{:S(2)}) copy-start(bf16[64,640]{1,0:T(8,128)(2,1)} %param.22) | copy-start | bytes 245764
  230.2 13.3 %copy-start.2 = (bf16[64,640]{1,0:T(8,128)(2,1)S(1)}, bf16[64,640]{1,0:T(8,128)(2,1)}, u32[]{:S(2)}) copy-start(bf16[64,640]{1,0:T(8,128)(2,1)} %param.21) | copy-start | bytes 245764
  230.2 14.0 %copy-start.8 = (f32[2,640]{1,0:T(2,128)S(1)}, f32[2,640]{1,0:T(2,128)}, u32[]{:S(2)}) copy-start(f32[2,640]{1,0:T(2,128)} %param.24) | copy-start | bytes 15364
  230.2 14.1 %copy-start.5 = (f32[2,3,640]{2,0,1:T(2,128)S(1)}, f32[2,3,640]{2,0,1:T(2,128)}, u32[]{:S(2)}) copy-start(f32[2,3,640]{2,0,1:T(2,128)} %param.23) | copy-start | bytes 46084
  230.2 326.2 %all-to-all-start.3 = ((bf16[32,640,64]{1,2,0:T(8,128)(2,1)}), bf16[32,640,64]{1,2,0:T(8,128)(2,1)}, u32[]{:S(2)}, u32[]{:S(2)}) async-start(bf16[32,640,64]{1,2,0:T(8,128)(2,1)} %stack.2), calls=%async_computation.3 | async-start | bytes 5242880 | tf_op jit(solution)/shard_map/all_to_all | solution.py:108
  243.2 1.6 copy-start.7
  243.2 307.4 %all-gather.5.cloned.1.call-start = ((), (), s32[]{:S(2)}) async-start(), calls=%async_computation.6 | async-start | bytes 5406720 | tf_op jit(solution)/shard_map/all_gather | solution.py:12
  550.6 3.4 copy-start.10
Sparse Core Ops, SparseCore 0:
  9.4 140.0 all-gather.2
  246.1 304.4 all-gather.4
